TPU v7x, 32 devices: a whole 2x2x4 slice. The times are simulated.
32 devices in a mesh: sp: 16 (over z, y, x), tp: 2 (over core).
Axes of the slice: x: 2, y: 2, z: 4, core: 2. Of those that a mesh axis runs over, the one named last changes fastest.
Arguments:
- stream: bfloat16 [7168, 2048], P('sp'), may hold values from -6 to 6
- norm_gain: float32 [2, 2048], replicated, may hold values from 0.1 to 1.9
- value_weight: bfloat16 [2, 2048, 512], P(None, None, 'tp'), may hold values from -0.125 to 0.125
- gate_weight: bfloat16 [2, 2048, 512], P(None, None, 'tp'), may hold values from -0.125 to 0.125
- conv_taps: bfloat16 [2, 512, 512], P(None, None, 'tp'), may hold values from -0.25 to 0.25
- conv_bias: float32 [2, 512], P(None, 'tp'), may hold values from -3 to 3
- channel_gain: float32 [2, 512], replicated, may hold values from 0.1 to 1.9
- channel_shift: float32 [2, 512], replicated, may hold values from -3 to 3
- out_weight: bfloat16 [2, 512, 2048], replicated, may hold values from -0.25 to 0.25
Outputs:
- result: bfloat16 [7168, 2048], P('sp')
All inputs are finite; a program needn't handle non-finite values.
Results may differ from a plain program's by a relative error of at most 0.0075.
Values may be sent and summed in bfloat16 or wider, within the bound.
A program may use at most 64 MiB of HBM per device.

v0:
```python
import functools

import jax
import jax.numpy as jnp
import numpy as np
from jax import lax
from jax.experimental import pallas as pl
from jax.experimental.pallas import tpu as pltpu
from jax.sharding import PartitionSpec as P

BLOCK = 128
MESH = pl.DeviceIdType.MESH


def dft_matrices(block):
    span = 2 * block
    angle = 2 * np.pi / span * np.outer(np.arange(block) + 0.5, np.arange(span))
    forward = np.concatenate([np.cos(angle), -np.sin(angle)], axis=0)
    of_taps = forward[:, block - 1 :: -1]
    inverse = forward[:, block:].T / block
    of_taps = np.concatenate([of_taps, np.zeros_like(of_taps)], axis=1)
    return jnp.asarray(np.concatenate([forward, inverse, of_taps]), jnp.bfloat16)


class Plan:
    def __init__(self, tokens, width, reach, n_sp):
        self.tokens, self.n_sp = tokens, n_sp
        self.parts = reach // BLOCK
        self.outs = -(-tokens // BLOCK)
        self.rows = (self.parts + self.outs) * BLOCK
        self.own = self.rows - tokens
        low = self.own - reach
        self.chunks = []
        for p in reversed(range(self.outs)):
            start = (self.parts + p) * BLOCK
            self.chunks.append((max(start, self.own), start + BLOCK))
        self.groups = [[c] for c in range(self.outs - 2)] + [list(range(max(self.outs - 2, 0), self.outs))]
        self.pieces = []
        for c, (a, b) in enumerate(self.chunks):
            for hop in range(1, min(-(-reach // tokens), n_sp - 1) + 1):
                first, end = max(a, low + hop * tokens) - hop * tokens, b - hop * tokens
                while first < end:
                    cut = max(first, (end - 1) // BLOCK * BLOCK if end <= self.outs * BLOCK else first)
                    when = c if hop == 1 else max(self.outs - 3, 0)
                    self.pieces.append((when, hop, cut + hop * tokens, cut, end - cut))
                    end = cut
        self.pieces.sort(key=lambda piece: piece[:2])
        self.needs = []
        for _, _, _, target, count in self.pieces:
            for g, group in enumerate(self.groups):
                if target + count > (self.outs - 1 - group[-1]) * BLOCK:
                    self.needs.append(g)
                    break


def scoped(fn):
    def named(*args):
        label = "_".join(str(a) for a in args if isinstance(a, (int, list)))
        with jax.named_scope(f"{fn.__name__}#{label}"):
            return fn(*args)

    return named


def kernel(
    plan, layers, stream, gain, wv, wg, taps, bias, cgain, cshift, wo, mats, x_v, mixed_v, wo_last,
    gain_v, w_v, taps_v, bias_v, cgain_v, cshift_v, wo_v, mats_v,
    gated, gained, spectra, kernels, freq, conv, peer, load_sem, send_sem, recv_sem, swap_send, swap_recv,
):
    sp, tp = lax.axis_index("sp"), lax.axis_index("tp")
    half = wv.shape[2]
    width = x_v.shape[1]
    mine = pl.ds(pl.multiple_of(tp * half, half), half)
    other = pl.ds(pl.multiple_of((1 - tp) * half, half), half)
    first, second = pl.ds(0, half), pl.ds(half, half)
    loads = {}
    waited = set()

    def load(key, whole, *parts):
        sem = load_sem.at[len(loads)]
        loads[key] = pltpu.make_async_copy(whole, whole, sem)
        for source, target in parts:
            pltpu.make_async_copy(source, target, sem).start()

    def need(*keys):
        for key in keys:
            if key not in waited:
                waited.add(key)
                loads[key].wait()

    def own_rows(c):
        a, b = plan.chunks[c]
        return pl.ds(a - plan.own, b - a)

    def load_rows(key, a, b):
        rows = pl.ds(a, b - a)
        load(key, x_v.at[rows], (stream.at[rows], x_v.at[rows]))

    def load_gate(l):
        load(("gate", l), w_v.at[l], (wv.at[l], w_v.at[l, :, first]), (wg.at[l], w_v.at[l, :, second]))

    def load_halves(key, source, target):
        load(key, target, (source(mine), target.at[first]), (source(other), target.at[second]))

    head = plan.chunks[0][0] - plan.own
    load("gain", gain_v, (gain, gain_v))
    load_rows("x0", head, x_v.shape[0])
    load_gate(0)
    load_rows("x", 0, head)
    load("taps", taps_v, (taps, taps_v))
    load("mats", mats_v, (mats, mats_v))
    load("bias", bias_v, (bias, bias_v))
    load("cgain", cgain_v, (cgain.at[:, mine], cgain_v.at[:, first]), (cgain.at[:, other], cgain_v.at[:, second]))
    load("cshift", cshift_v, (cshift.at[:, mine], cshift_v.at[:, first]), (cshift.at[:, other], cshift_v.at[:, second]))
    for l in range(layers):
        if l:
            load_gate(l)
        load_halves(("out", l), lambda channels: wo.at[l, channels], wo_last if l == layers - 1 else wo_v.at[l])
    fwd_v, inv_v = mats_v.at[: 2 * BLOCK], mats_v.at[2 * BLOCK : 3 * BLOCK]
    oft_v = mats_v.at[3 * BLOCK :, :BLOCK]

    for l in range(layers):
        gated[l, : plan.own] = jnp.zeros((plan.own, half), jnp.bfloat16)

    hops = sorted({piece[1] for piece in plan.pieces})
    barrier = pltpu.get_barrier_semaphore()
    pl.semaphore_signal(barrier, inc=1, device_id={"tp": 1 - tp}, device_id_type=MESH)
    for hop in hops:
        @pl.when(sp >= hop)
        def _():
            pl.semaphore_signal(barrier, inc=1, device_id={"sp": sp - hop}, device_id_type=MESH)

    def piece_copy(l, i):
        _, hop, source, target, count = plan.pieces[i]
        return pltpu.make_async_remote_copy(
            src_ref=gated.at[l, pl.ds(source, count)],
            dst_ref=gated.at[l, pl.ds(target, count)],
            send_sem=send_sem.at[hops.index(hop)],
            recv_sem=recv_sem.at[l, hops.index(hop), plan.needs[i]],
            device_id={"sp": sp + hop},
            device_id_type=MESH,
        )

    group_of = {c: g for g, group in enumerate(plan.groups) for c in group}

    def swap_copy(l, c):
        return pltpu.make_async_remote_copy(
            src_ref=conv.at[l, own_rows(c)],
            dst_ref=peer.at[l, own_rows(c)],
            send_sem=swap_send.at[0],
            recv_sem=swap_recv.at[l, group_of[c]],
            device_id={"tp": 1 - tp},
            device_id_type=MESH,
        )

    def span(group):
        return plan.chunks[group[-1]][0], plan.chunks[group[0]][1]

    def span_rows(group):
        a, b = span(group)
        return pl.ds(a - plan.own, b - a)

    @scoped
    def gate(l, group, squares=None):
        rows = span_rows(group)
        if squares is None:
            need("gain", "x" if group[0] else "x0")
            squares = 0.0
            step = width // 4
            for k in range(0, width, step):
                x = x_v[rows, k : k + step].astype(jnp.float32)
                squares = squares + jnp.sum(x * x, axis=-1, keepdims=True)
                gained[rows, k : k + step] = (x * gain_v[l : l + 1, k : k + step]).astype(jnp.bfloat16)
        need(("gate", l))
        both = jnp.dot(gained[rows, :], w_v[l], preferred_element_type=jnp.float32)
        both = both * lax.rsqrt(squares / width + 1e-06)
        a, b = span(group)
        gated[l, a:b, :] = (both[:, :half] * jax.nn.sigmoid(both[:, half:])).astype(jnp.bfloat16)

    @scoped
    def send(l, c):
        for i, piece in enumerate(plan.pieces):
            if piece[0] == c:
                @pl.when(sp + piece[1] < plan.n_sp)
                def _():
                    piece_copy(l, i).start()

    @scoped
    def transform_taps(l):
        need("taps", "mats")
        for j in range(plan.parts):
            first = (plan.parts - 1 - j) * BLOCK
            kernels[l, j] = jnp.dot(
                oft_v[...], taps_v[l, first : first + BLOCK, :], preferred_element_type=jnp.float32
            )

    def whole(ref, sem):
        return pltpu.make_async_copy(ref, ref, sem)

    def await_group(l, g):
        for h, hop in enumerate(hops):
            spans = [(piece[3], piece[3] + piece[4]) for i, piece in enumerate(plan.pieces) if plan.needs[i] == g and piece[1] == hop]
            if spans:
                low, high = min(a for a, _ in spans), max(b for _, b in spans)
                assert high - low == sum(b - a for a, b in spans)
                with jax.named_scope(f"recv{hop}_{g}"):
                    @pl.when(sp >= hop)
                    def _():
                        whole(gated.at[l, pl.ds(low, high - low)], recv_sem.at[l, h, g]).wait()

    @scoped
    def spectrum(l, w):
        first, last = w * BLOCK, (w + 2) * BLOCK
        spectra[l, w] = jnp.dot(fwd_v[...], gated[l, first:last, :], preferred_element_type=jnp.float32)

    def mix_bins(l, c):
        p = plan.outs - 1 - c
        tile = 16
        for k in range(0, BLOCK, tile):
            low, high = slice(k, k + tile), slice(BLOCK + k, BLOCK + k + tile)
            real = imag = None
            for j in range(plan.parts):
                w = plan.parts - 1 + p - j
                xr, xi = spectra[l, w, low, :], spectra[l, w, high, :]
                hr, hi = kernels[l, j, low, :], kernels[l, j, high, :]
                r, i = xr * hr - xi * hi, xr * hi + xi * hr
                real, imag = (r, i) if real is None else (real + r, imag + i)
            freq[c, low, :] = real.astype(jnp.bfloat16)
            freq[c, high, :] = imag.astype(jnp.bfloat16)

    def invert(l, c):
        a, b = plan.chunks[c]
        result = jnp.dot(inv_v[BLOCK - (b - a) :, :], freq[c], preferred_element_type=jnp.float32)
        conv[l, own_rows(c), :] = (result + bias_v[l : l + 1, :]).astype(jnp.bfloat16)
        swap_copy(l, c).start()

    transformed = set()

    def spectra_for(l, group, own):
        p = plan.outs - 1 - group[-1]
        q = plan.outs - 1 - group[0]
        fresh = [w for w in range(p, q + plan.parts) if (l, w) not in transformed]
        fresh = [w for w in reversed(fresh) if not own or w * BLOCK >= plan.own]
        if not own:
            await_group(l, group_of[group[0]])
        for w in fresh:
            transformed.add((l, w))
            spectrum(l, w)

    @scoped
    def convolve(l, group):
        for c in group:
            mix_bins(l, c)
        for c in group:
            invert(l, c)

    def await_swap(l, group):
        with jax.named_scope("swapwait"):
            whole(peer.at[l, span_rows(group)], swap_recv.at[l, group_of[group[0]]]).wait()

    def mix(l, group):
        rows = span_rows(group)
        need("cgain", "cshift")
        values = jnp.concatenate([conv[l, rows, :], peer[l, rows, :]], axis=-1).astype(jnp.float32)
        center = jnp.mean(values, axis=-1, keepdims=True)
        values = values - center
        spread = jnp.mean(values * values, axis=-1, keepdims=True)
        normed = values * lax.rsqrt(spread + 1e-05) * cgain_v[l : l + 1, :] + cshift_v[l : l + 1, :]
        return (normed * jax.nn.sigmoid(normed)).astype(jnp.bfloat16)

    @scoped
    def finish(l, group):
        rows = span_rows(group)
        last = l == layers - 1
        await_swap(l, group)
        need("cgain", "cshift", ("out", l))
        if not last:
            need(("gate", l + 1))
        mixed = mix(l, group)
        out = wo_last if last else wo_v.at[l]
        step = width // 4
        squares = 0.0
        for n in range(0, width, step):
            update = jnp.dot(mixed, out[:, n : n + step], preferred_element_type=jnp.float32)
            new = (x_v[rows, n : n + step].astype(jnp.float32) + update).astype(jnp.bfloat16)
            x_v[rows, n : n + step] = new
            if not last:
                x = new.astype(jnp.float32)
                squares = squares + jnp.sum(x * x, axis=-1, keepdims=True)
                gained[rows, n : n + step] = (x * gain_v[l + 1 : l + 2, n : n + step]).astype(jnp.bfloat16)
        if not last:
            gate(l + 1, group, squares)
            for c in group:
                send(l + 1, c)

    for c in range(plan.outs):
        gate(0, [c])
        if c == 0:
            with jax.named_scope("barrier"):
                pl.semaphore_wait(barrier, 1 + jnp.minimum(plan.n_sp - 1 - sp, len(hops)))
        send(0, c)
    for l in range(layers):
        transform_taps(l)
    need("bias")
    for l in range(layers):
        spectra_for(l, plan.groups[0], True)
        finished = 0
        for g, group in enumerate(plan.groups):
            spectra_for(l, group, False)
            convolve(l, group)
            if g:
                finish(l, plan.groups[finished])
                finished += 1
        for group in plan.groups[finished:-1] if l == layers - 1 else plan.groups[finished:]:
            finish(l, group)

    await_swap(layers - 1, plan.groups[-1])
    mixed_v[...] = mix(layers - 1, plan.groups[-1])
    whole(conv, swap_send.at[0]).wait()
    for h, hop in enumerate(hops):
        count = sum(piece[4] for piece in plan.pieces if piece[1] == hop)

        @pl.when(sp + hop < plan.n_sp)
        def _():
            whole(gated.at[:, pl.ds(0, count)], send_sem.at[h]).wait()


def last_out(done, x_v, mixed, wo, result, tail, sem):
    rows, width = tail.shape
    copies = [pltpu.make_async_copy(x_v.at[a:b], result.at[a:b], sem.at[0]) for a, b in done]
    for copy in copies:
        copy.start()
    step = width // 4
    for n in range(0, width, step):
        update = jnp.dot(mixed[...], wo[:, n : n + step], preferred_element_type=jnp.float32)
        tail[:, n : n + step] = (x_v[:rows, n : n + step].astype(jnp.float32) + update).astype(jnp.bfloat16)
        copy = pltpu.make_async_copy(tail.at[:, n : n + step], result.at[:rows, n : n + step], sem.at[0])
        copy.start()
        copies.append(copy)
    for copy in copies:
        copy.wait()


def per_device(stream, norm_gain, value_weight, gate_weight, conv_taps, conv_bias, channel_gain, channel_shift, out_weight):
    tokens, width = stream.shape
    layers, reach, half = conv_taps.shape
    plan = Plan(tokens, width, reach, lax.axis_size("sp"))
    mats = dft_matrices(BLOCK)
    n_hops = len({piece[1] for piece in plan.pieces})
    bf16, f32, dma = jnp.bfloat16, jnp.float32, pltpu.SemaphoreType.DMA
    windows = plan.parts + plan.outs - 1
    last_rows = sum(b - a for a, b in (plan.chunks[c] for c in plan.groups[-1]))
    x, mixed, wo_last = pl.pallas_call(
        functools.partial(kernel, plan, layers),
        out_shape=[
            pltpu.VMEM(stream.shape, stream.dtype),
            pltpu.VMEM((last_rows, 2 * half), bf16),
            pltpu.VMEM(out_weight.shape[1:], bf16),
        ],
        in_specs=[pl.BlockSpec(memory_space=pltpu.HBM)] * 10,
        out_specs=[pl.BlockSpec(memory_space=pltpu.VMEM)] * 3,
        scratch_shapes=[
            pltpu.VMEM(norm_gain.shape, f32),
            pltpu.VMEM((layers, width, 2 * half), bf16),
            pltpu.VMEM(conv_taps.shape, bf16),
            pltpu.VMEM(conv_bias.shape, f32),
            pltpu.VMEM(channel_gain.shape, f32),
            pltpu.VMEM(channel_shift.shape, f32),
            pltpu.VMEM((layers - 1, *out_weight.shape[1:]), bf16),
            pltpu.VMEM(mats.shape, bf16),
            pltpu.VMEM((layers, plan.rows, half), bf16),
            pltpu.VMEM((tokens, width), bf16),
            pltpu.VMEM((layers, windows, 2 * BLOCK, half), f32),
            pltpu.VMEM((layers, plan.parts, 2 * BLOCK, half), f32),
            pltpu.VMEM((plan.outs, 2 * BLOCK, half), bf16),
            pltpu.VMEM((layers, tokens, half), bf16),
            pltpu.VMEM((layers, tokens, half), bf16),
            dma((8 + 2 * layers,)),
            dma((n_hops,)),
            dma((layers, n_hops, len(plan.groups))),
            dma((1,)),
            dma((layers, len(plan.groups))),
        ],
        compiler_params=pltpu.CompilerParams(
            collective_id=0, has_side_effects=True, vmem_limit_bytes=61400 * 1024
        ),
    )(stream, norm_gain, value_weight, gate_weight, conv_taps, conv_bias, channel_gain, channel_shift, out_weight, mats)
    done = [(plan.chunks[c][0] - plan.own, plan.chunks[c][1] - plan.own) for g in plan.groups[:-1] for c in g]
    return pl.pallas_call(
        functools.partial(last_out, done),
        out_shape=jax.ShapeDtypeStruct(stream.shape, stream.dtype),
        in_specs=[pl.BlockSpec(memory_space=pltpu.VMEM)] * 3,
        out_specs=pl.BlockSpec(memory_space=pltpu.HBM),
        scratch_shapes=[pltpu.VMEM((last_rows, width), bf16), dma((1,))],
        compiler_params=pltpu.CompilerParams(vmem_limit_bytes=16000 * 1024),
    )(x, mixed, wo_last)


def solution(mesh):
    return jax.shard_map(
        per_device,
        mesh=mesh,
        in_specs=(
            P("sp", None),
            P(),
            P(None, None, "tp"),
            P(None, None, "tp"),
            P(None, None, "tp"),
            P(None, "tp"),
            P(),
            P(),
            P(),
        ),
        out_specs=P("sp", None),
        check_vma=False,
    )
```

profile of v0, /device:TPU:25, one launch (start us, length us, event | category | flops | bytes accessed | tf_op | source)
XLA Modules:
  0.0 22.3 jit_solution(12786779053234666137)
XLA Ops:
  0.0 21.0 %shard_map.100 = (bf16[448,2048]{1,0:T(8,128)(2,1)S(1)}, bf16[192,512]{1,0:T(8,128)(2,1)S(1)}, bf16[512,2048]{1,0:T(8,128)(2,1)S(1)}) custom-call(bf16[448,2048]{1,0:T(8,128)(2,1)} %stream.1, f32[2,2048]{1,0:T(2,128)} %gain.1, bf16[2,2048,256]{2,1,0:T(8,128)(2,1)} %wv.1, bf16[2,2048,256]{2,1,0:T(8,128)(2,1)} %wg.1, bf16[2,512,256]{2,1,0:T(8,128)(2,1)} %taps.1, ...), custom_call_target="tpu_custom_call" | custom-call | tf_op jit(solution)/shard_map/pallas_call | solution.py:353
  21.0 1.3 %shard_map.101 = bf16[448,2048]{1,0:T(8,128)(2,1)} custom-call(bf16[448,2048]{1,0:T(8,128)(2,1)S(1)} %get-tuple-element.8.x_v, bf16[192,512]{1,0:T(8,128)(2,1)S(1)} %get-tuple-element.9.mixed, bf16[512,2048]{1,0:T(8,128)(2,1)S(1)} %get-tuple-element.10.wo), custom_call_target="tpu_custom_call" | custom-call | tf_op jit(solution)/shard_map/pallas_call | solution.py:389
where the time goes:
time: 22.6 us; the launch traced here: 22.3 us
  Pallas kernels  22.3 us (99%)
    pallas_call x1, Pallas kernels, per_device(): pl.pallas_call(functools.partial(kernel, plan, layers), out_shape=[pltpu....  21 us
    pallas_call x1, Pallas kernels, per_device(): pl.pallas_call(functools.partial(last_out, done), out_shape=jax.ShapeDtyp...  1.28 us

commit v1 on v0

--- a/solution.py
+++ b/solution.py
@@ -9,6 +9,8 @@
 from jax.sharding import PartitionSpec as P
 
 BLOCK = 128
+STEPS = 4
+LANES = 128
 MESH = pl.DeviceIdType.MESH
 
 
@@ -65,7 +67,7 @@
 def kernel(
     plan, layers, stream, gain, wv, wg, taps, bias, cgain, cshift, wo, mats, x_v, mixed_v, wo_last,
     gain_v, w_v, taps_v, bias_v, cgain_v, cshift_v, wo_v, mats_v,
-    gated, gained, spectra, kernels, freq, conv, peer, load_sem, send_sem, recv_sem, swap_send, swap_recv,
+    gated, gained, spectra, kernels, sums, freq, conv, peer, shift, load_sem, send_sem, recv_sem, swap_send, swap_recv, fence_sem,
 ):
     sp, tp = lax.axis_index("sp"), lax.axis_index("tp")
     half = wv.shape[2]
@@ -96,8 +98,11 @@
         rows = pl.ds(a, b - a)
         load(key, x_v.at[rows], (stream.at[rows], x_v.at[rows]))
 
-    def load_gate(l):
-        load(("gate", l), w_v.at[l], (wv.at[l], w_v.at[l, :, first]), (wg.at[l], w_v.at[l, :, second]))
+    def load_gate(l, steps=1):
+        for k in range(steps):
+            depth = pl.ds(k * (width // steps), width // steps)
+            parts = (wv.at[l, depth], w_v.at[l, depth, first]), (wg.at[l, depth], w_v.at[l, depth, second])
+            load(("gate", l, k), w_v.at[l, depth], *parts)
 
     def load_halves(key, source, target):
         load(key, target, (source(mine), target.at[first]), (source(other), target.at[second]))
@@ -105,7 +110,7 @@
     head = plan.chunks[0][0] - plan.own
     load("gain", gain_v, (gain, gain_v))
     load_rows("x0", head, x_v.shape[0])
-    load_gate(0)
+    load_gate(0, STEPS)
     load_rows("x", 0, head)
     load("taps", taps_v, (taps, taps_v))
     load("mats", mats_v, (mats, mats_v))
@@ -171,8 +176,14 @@
                 x = x_v[rows, k : k + step].astype(jnp.float32)
                 squares = squares + jnp.sum(x * x, axis=-1, keepdims=True)
                 gained[rows, k : k + step] = (x * gain_v[l : l + 1, k : k + step]).astype(jnp.bfloat16)
-        need(("gate", l))
-        both = jnp.dot(gained[rows, :], w_v[l], preferred_element_type=jnp.float32)
+        if l == 0 and ("gate", 0, STEPS - 1) not in waited:
+            both = 0.0
+            for k in range(STEPS):
+                depth = slice(k * (width // STEPS), (k + 1) * (width // STEPS))
+                need(("gate", 0, k))
+                both = both + jnp.dot(gained[rows, depth], w_v[l, depth], preferred_element_type=jnp.float32)
+        else:
+            both = jnp.dot(gained[rows, :], w_v[l], preferred_element_type=jnp.float32)
         both = both * lax.rsqrt(squares / width + 1e-06)
         a, b = span(group)
         gated[l, a:b, :] = (both[:, :half] * jax.nn.sigmoid(both[:, half:])).astype(jnp.bfloat16)
@@ -213,20 +224,45 @@
         first, last = w * BLOCK, (w + 2) * BLOCK
         spectra[l, w] = jnp.dot(fwd_v[...], gated[l, first:last, :], preferred_element_type=jnp.float32)
 
-    def mix_bins(l, c):
+    summed = {}
+
+    def add_bins(l, c, windows, final=False):
         p = plan.outs - 1 - c
+        begun = (l, c) in summed
+        summed[l, c] = True
         tile = 16
         for k in range(0, BLOCK, tile):
             low, high = slice(k, k + tile), slice(BLOCK + k, BLOCK + k + tile)
-            real = imag = None
-            for j in range(plan.parts):
-                w = plan.parts - 1 + p - j
+            real, imag = (sums[c, low, :], sums[c, high, :]) if begun else (None, None)
+            for w in windows:
+                j = plan.parts - 1 + p - w
                 xr, xi = spectra[l, w, low, :], spectra[l, w, high, :]
                 hr, hi = kernels[l, j, low, :], kernels[l, j, high, :]
                 r, i = xr * hr - xi * hi, xr * hi + xi * hr
                 real, imag = (r, i) if real is None else (real + r, imag + i)
-            freq[c, low, :] = real.astype(jnp.bfloat16)
-            freq[c, high, :] = imag.astype(jnp.bfloat16)
+            if final:
+                freq[c, low, :] = real.astype(jnp.bfloat16)
+                freq[c, high, :] = imag.astype(jnp.bfloat16)
+            else:
+                sums[c, low, :], sums[c, high, :] = real, imag
+
+    unused = {(l, c): [w for w in reversed(range(plan.outs - 1 - c, plan.outs - 1 - c + plan.parts))] for l in range(layers) for c in range(plan.outs)}
+
+    def add_ready(l, c, final=False):
+        ready = [w for w in unused[l, c] if (l, w) in transformed]
+        unused[l, c] = [w for w in unused[l, c] if w not in ready]
+        assert not (final and unused[l, c])
+        if ready or final:
+            add_bins(l, c, ready, final)
+
+    def add_later(l, groups):
+        for group in groups:
+            for c in group:
+                add_ready(l, c)
+
+    def fence():
+        pl.semaphore_signal(fence_sem, 1)
+        pl.semaphore_wait(fence_sem, 1)
 
     def invert(l, c):
         a, b = plan.chunks[c]
@@ -250,32 +286,41 @@
     @scoped
     def convolve(l, group):
         for c in group:
-            mix_bins(l, c)
+            add_ready(l, c, final=True)
         for c in group:
             invert(l, c)
 
     def await_swap(l, group):
         with jax.named_scope("swapwait"):
             whole(peer.at[l, span_rows(group)], swap_recv.at[l, group_of[group[0]]]).wait()
+
+    def own_mean(l, group):
+        rows = span_rows(group)
+        mean = jnp.mean(conv[l, rows, :].astype(jnp.float32), axis=-1, keepdims=True)
+        shift[l, rows, :] = jnp.broadcast_to(mean, (mean.shape[0], LANES))
 
     def mix(l, group):
         rows = span_rows(group)
         need("cgain", "cshift")
         values = jnp.concatenate([conv[l, rows, :], peer[l, rows, :]], axis=-1).astype(jnp.float32)
-        center = jnp.mean(values, axis=-1, keepdims=True)
-        values = values - center
-        spread = jnp.mean(values * values, axis=-1, keepdims=True)
-        normed = values * lax.rsqrt(spread + 1e-05) * cgain_v[l : l + 1, :] + cshift_v[l : l + 1, :]
+        channels = values.shape[1]
+        values = values - jnp.concatenate([shift[l, rows, :]] * (channels // LANES), axis=-1)
+        center = jnp.sum(values, axis=-1, keepdims=True) / channels
+        spread = jnp.sum(values * values, axis=-1, keepdims=True) / channels - center * center
+        scale = lax.rsqrt(jnp.maximum(spread, 0.0) + 1e-05)
+        normed = (values - center) * scale * cgain_v[l : l + 1, :] + cshift_v[l : l + 1, :]
         return (normed * jax.nn.sigmoid(normed)).astype(jnp.bfloat16)
 
     @scoped
-    def finish(l, group):
+    def finish(l, group, after=None):
         rows = span_rows(group)
         last = l == layers - 1
         await_swap(l, group)
         need("cgain", "cshift", ("out", l))
         if not last:
-            need(("gate", l + 1))
+            need(("gate", l + 1, 0))
+        if after:
+            own_mean(l, after)
         mixed = mix(l, group)
         out = wo_last if last else wo_v.at[l]
         step = width // 4
@@ -290,6 +335,8 @@
                 gained[rows, n : n + step] = (x * gain_v[l + 1 : l + 2, n : n + step]).astype(jnp.bfloat16)
         if not last:
             gate(l + 1, group, squares)
+        add_later(l, plan.groups)
+        if not last:
             for c in group:
                 send(l + 1, c)
 
@@ -303,16 +350,21 @@
         transform_taps(l)
     need("bias")
     for l in range(layers):
+        last = l == layers - 1
         spectra_for(l, plan.groups[0], True)
-        finished = 0
+        add_later(l, plan.groups)
         for g, group in enumerate(plan.groups):
             spectra_for(l, group, False)
+            if g:
+                own_mean(l, plan.groups[g - 1])
             convolve(l, group)
-            if g:
-                finish(l, plan.groups[finished])
-                finished += 1
-        for group in plan.groups[finished:-1] if l == layers - 1 else plan.groups[finished:]:
-            finish(l, group)
+            if g == 0:
+                fence()
+                add_later(l, plan.groups[1:])
+            else:
+                finish(l, plan.groups[g - 1], group if group is plan.groups[-1] else None)
+        if not last:
+            finish(l, plan.groups[-1])
 
     await_swap(layers - 1, plan.groups[-1])
     mixed_v[...] = mix(layers - 1, plan.groups[-1])
@@ -372,14 +424,17 @@
             pltpu.VMEM((tokens, width), bf16),
             pltpu.VMEM((layers, windows, 2 * BLOCK, half), f32),
             pltpu.VMEM((layers, plan.parts, 2 * BLOCK, half), f32),
+            pltpu.VMEM((plan.outs, 2 * BLOCK, half), f32),
             pltpu.VMEM((plan.outs, 2 * BLOCK, half), bf16),
             pltpu.VMEM((layers, tokens, half), bf16),
             pltpu.VMEM((layers, tokens, half), bf16),
-            dma((8 + 2 * layers,)),
+            pltpu.VMEM((layers, tokens, LANES), f32),
+            dma((7 + STEPS + 2 * layers,)),
             dma((n_hops,)),
             dma((layers, n_hops, len(plan.groups))),
             dma((1,)),
             dma((layers, len(plan.groups))),
+            pltpu.SemaphoreType.REGULAR,
         ],
         compiler_params=pltpu.CompilerParams(
             collective_id=0, has_side_effects=True, vmem_limit_bytes=61400 * 1024

time: 22.6 us -> 22.1 us (0.978)
  Pallas kernels: 22.3 us -> 21.8 us
    pallas_call x1, Pallas kernels: 21 us -> 20.6 us  [per_device(): pl.pallas_call(functools.partial(kernel, plan, layers), out_shape=[pltpu....]
where the time goes in v1:
time: 22.1 us; the launch traced here: 21.8 us
  Pallas kernels  21.8 us (99%)
    pallas_call x1, Pallas kernels, per_device(): pl.pallas_call(functools.partial(kernel, plan, layers), out_shape=[pltpu....  20.6 us
    pallas_call x1, Pallas kernels, per_device(): pl.pallas_call(functools.partial(last_out, done), out_shape=jax.ShapeDtyp...  1.28 us

profile of v1, /device:TPU:25, one launch (start us, length us, event | category | flops | bytes accessed | tf_op | source)
XLA Modules:
  0.0 21.8 jit_solution(11325258023040280011)
XLA Ops:
  0.0 20.6 %shard_map.100 = (bf16[448,2048]{1,0:T(8,128)(2,1)S(1)}, bf16[192,512]{1,0:T(8,128)(2,1)S(1)}, bf16[512,2048]{1,0:T(8,128)(2,1)S(1)}) custom-call(bf16[448,2048]{1,0:T(8,128)(2,1)} %stream.1, f32[2,2048]{1,0:T(2,128)} %gain.1, bf16[2,2048,256]{2,1,0:T(8,128)(2,1)} %wv.1, bf16[2,2048,256]{2,1,0:T(8,128)(2,1)} %wg.1, bf16[2,512,256]{2,1,0:T(8,128)(2,1)} %taps.1, ...), custom_call_target="tpu_custom_call" | custom-call | tf_op jit(solution)/shard_map/pallas_call | solution.py:405
  20.6 1.3 %shard_map.101 = bf16[448,2048]{1,0:T(8,128)(2,1)} custom-call(bf16[448,2048]{1,0:T(8,128)(2,1)S(1)} %get-tuple-element.8.x_v, bf16[192,512]{1,0:T(8,128)(2,1)S(1)} %get-tuple-element.9.mixed, bf16[512,2048]{1,0:T(8,128)(2,1)S(1)} %get-tuple-element.10.wo), custom_call_target="tpu_custom_call" | custom-call | tf_op jit(solution)/shard_map/pallas_call | solution.py:444

commit v2 on v1

--- a/solution.py
+++ b/solution.py
@@ -10,6 +10,8 @@
 
 BLOCK = 128
 STEPS = 4
+ORDER = [("conv", [0]), ("conv", [1]), ("out", [0]), ("conv", [2]), ("out", [1]), ("conv", [3]), ("out", [2]), ("out", [3])]
+ORDER_LAST = [("conv", [0]), ("conv", [1]), ("out", [0]), ("conv", [2]), ("conv", [3]), ("out", [1]), ("out", [2])]
 LANES = 128
 MESH = pl.DeviceIdType.MESH
 
@@ -30,19 +32,20 @@
         self.parts = reach // BLOCK
         self.outs = -(-tokens // BLOCK)
         self.rows = (self.parts + self.outs) * BLOCK
-        self.own = self.rows - tokens
+        self.own = self.parts * BLOCK
         low = self.own - reach
         self.chunks = []
         for p in reversed(range(self.outs)):
             start = (self.parts + p) * BLOCK
-            self.chunks.append((max(start, self.own), start + BLOCK))
-        self.groups = [[c] for c in range(self.outs - 2)] + [list(range(max(self.outs - 2, 0), self.outs))]
+            self.chunks.append((start, min(start + BLOCK, self.own + tokens)))
+        self.groups = [[c] for c in range(self.outs)]
+        self.tail = list(range(max(self.outs - 1, 0), self.outs))
         self.pieces = []
         for c, (a, b) in enumerate(self.chunks):
             for hop in range(1, min(-(-reach // tokens), n_sp - 1) + 1):
                 first, end = max(a, low + hop * tokens) - hop * tokens, b - hop * tokens
                 while first < end:
-                    cut = max(first, (end - 1) // BLOCK * BLOCK if end <= self.outs * BLOCK else first)
+                    cut = max(first, (end - 1) // BLOCK * BLOCK if hop == 1 else first)
                     when = c if hop == 1 else max(self.outs - 3, 0)
                     self.pieces.append((when, hop, cut + hop * tokens, cut, end - cut))
                     end = cut
@@ -53,6 +56,7 @@
                 if target + count > (self.outs - 1 - group[-1]) * BLOCK:
                     self.needs.append(g)
                     break
+        self.slots = sorted({(piece[1], need) for piece, need in zip(self.pieces, self.needs)})
 
 
 def scoped(fn):
@@ -125,7 +129,9 @@
     oft_v = mats_v.at[3 * BLOCK :, :BLOCK]
 
     for l in range(layers):
+        end = plan.own + x_v.shape[0]
         gated[l, : plan.own] = jnp.zeros((plan.own, half), jnp.bfloat16)
+        gated[l, end:] = jnp.zeros((plan.rows - end, half), jnp.bfloat16)
 
     hops = sorted({piece[1] for piece in plan.pieces})
     barrier = pltpu.get_barrier_semaphore()
@@ -141,7 +147,7 @@
             src_ref=gated.at[l, pl.ds(source, count)],
             dst_ref=gated.at[l, pl.ds(target, count)],
             send_sem=send_sem.at[hops.index(hop)],
-            recv_sem=recv_sem.at[l, hops.index(hop), plan.needs[i]],
+            recv_sem=recv_sem.at[l, plan.slots.index((hop, plan.needs[i]))],
             device_id={"sp": sp + hop},
             device_id_type=MESH,
         )
@@ -217,7 +223,7 @@
                 with jax.named_scope(f"recv{hop}_{g}"):
                     @pl.when(sp >= hop)
                     def _():
-                        whole(gated.at[l, pl.ds(low, high - low)], recv_sem.at[l, h, g]).wait()
+                        whole(gated.at[l, pl.ds(low, high - low)], recv_sem.at[l, plan.slots.index((hop, g))]).wait()
 
     @scoped
     def spectrum(l, w):
@@ -266,7 +272,7 @@
 
     def invert(l, c):
         a, b = plan.chunks[c]
-        result = jnp.dot(inv_v[BLOCK - (b - a) :, :], freq[c], preferred_element_type=jnp.float32)
+        result = jnp.dot(inv_v[: b - a, :], freq[c], preferred_element_type=jnp.float32)
         conv[l, own_rows(c), :] = (result + bias_v[l : l + 1, :]).astype(jnp.bfloat16)
         swap_copy(l, c).start()
 
@@ -311,16 +317,25 @@
         normed = (values - center) * scale * cgain_v[l : l + 1, :] + cshift_v[l : l + 1, :]
         return (normed * jax.nn.sigmoid(normed)).astype(jnp.bfloat16)
 
-    @scoped
-    def finish(l, group, after=None):
+    swapped = set()
+
+    @scoped
+    def finish(l, group, unmeaned):
         rows = span_rows(group)
         last = l == layers - 1
-        await_swap(l, group)
+        for g in sorted({group_of[c] for c in group}):
+            if (l, g) not in swapped:
+                swapped.add((l, g))
+                await_swap(l, plan.groups[g])
+        for part in unmeaned:
+            if group_of[part[0]] in {group_of[c] for c in group}:
+                own_mean(l, part)
         need("cgain", "cshift", ("out", l))
         if not last:
             need(("gate", l + 1, 0))
-        if after:
-            own_mean(l, after)
+        for part in unmeaned:
+            if group_of[part[0]] not in {group_of[c] for c in group}:
+                own_mean(l, part)
         mixed = mix(l, group)
         out = wo_last if last else wo_v.at[l]
         step = width // 4
@@ -350,24 +365,29 @@
         transform_taps(l)
     need("bias")
     for l in range(layers):
-        last = l == layers - 1
         spectra_for(l, plan.groups[0], True)
         add_later(l, plan.groups)
-        for g, group in enumerate(plan.groups):
-            spectra_for(l, group, False)
-            if g:
-                own_mean(l, plan.groups[g - 1])
-            convolve(l, group)
-            if g == 0:
-                fence()
-                add_later(l, plan.groups[1:])
+        unmeaned = []
+        for step, which in ORDER_LAST if l == layers - 1 else ORDER:
+            if step == "conv":
+                group = plan.groups[which[0]]
+                spectra_for(l, group, False)
+                for part in unmeaned:
+                    own_mean(l, part)
+                convolve(l, group)
+                unmeaned = [group]
+                if which == [0]:
+                    fence()
+                    add_later(l, plan.groups[1:])
             else:
-                finish(l, plan.groups[g - 1], group if group is plan.groups[-1] else None)
-        if not last:
-            finish(l, plan.groups[-1])
-
-    await_swap(layers - 1, plan.groups[-1])
-    mixed_v[...] = mix(layers - 1, plan.groups[-1])
+                finish(l, which, unmeaned)
+                unmeaned = []
+
+    for c in plan.tail:
+        await_swap(layers - 1, [c])
+        if [c] in unmeaned:
+            own_mean(layers - 1, [c])
+        mixed_v[own_rows(c)] = mix(layers - 1, [c])
     whole(conv, swap_send.at[0]).wait()
     for h, hop in enumerate(hops):
         count = sum(piece[4] for piece in plan.pieces if piece[1] == hop)
@@ -401,7 +421,7 @@
     n_hops = len({piece[1] for piece in plan.pieces})
     bf16, f32, dma = jnp.bfloat16, jnp.float32, pltpu.SemaphoreType.DMA
     windows = plan.parts + plan.outs - 1
-    last_rows = sum(b - a for a, b in (plan.chunks[c] for c in plan.groups[-1]))
+    last_rows = sum(b - a for a, b in (plan.chunks[c] for c in plan.tail))
     x, mixed, wo_last = pl.pallas_call(
         functools.partial(kernel, plan, layers),
         out_shape=[
@@ -431,16 +451,16 @@
             pltpu.VMEM((layers, tokens, LANES), f32),
             dma((7 + STEPS + 2 * layers,)),
             dma((n_hops,)),
-            dma((layers, n_hops, len(plan.groups))),
+            dma((layers, len(plan.slots))),
             dma((1,)),
             dma((layers, len(plan.groups))),
             pltpu.SemaphoreType.REGULAR,
         ],
         compiler_params=pltpu.CompilerParams(
-            collective_id=0, has_side_effects=True, vmem_limit_bytes=61400 * 1024
+            collective_id=0, has_side_effects=True, vmem_limit_bytes=61300 * 1024
         ),
     )(stream, norm_gain, value_weight, gate_weight, conv_taps, conv_bias, channel_gain, channel_shift, out_weight, mats)
-    done = [(plan.chunks[c][0] - plan.own, plan.chunks[c][1] - plan.own) for g in plan.groups[:-1] for c in g]
+    done = [(plan.chunks[c][0] - plan.own, plan.chunks[c][1] - plan.own) for c in range(plan.outs) if c not in plan.tail]
     return pl.pallas_call(
         functools.partial(last_out, done),
         out_shape=jax.ShapeDtypeStruct(stream.shape, stream.dtype),

time: 22.1 us -> 21.5 us (0.973)
  Pallas kernels: 21.8 us -> 21.2 us
    pallas_call x1, Pallas kernels: 20.6 us -> 20 us  [per_device(): pl.pallas_call(functools.partial(kernel, plan, layers), out_shape=[pltpu....]
where the time goes in v2:
time: 21.5 us; the launch traced here: 21.2 us
  Pallas kernels  21.2 us (99%)
    pallas_call x1, Pallas kernels, per_device(): pl.pallas_call(functools.partial(kernel, plan, layers), out_shape=[pltpu....  20 us
    pallas_call x1, Pallas kernels, per_device(): pl.pallas_call(functools.partial(last_out, done), out_shape=jax.ShapeDtyp...  1.22 us

profile of v2, /device:TPU:25, one launch (start us, length us, event | category | flops | bytes accessed | tf_op | source)
XLA Modules:
  0.0 21.2 jit_solution(17285785445410055107)
XLA Ops:
  0.0 20.0 %shard_map.100 = (bf16[448,2048]{1,0:T(8,128)(2,1)S(1)}, bf16[128,512]{1,0:T(8,128)(2,1)S(1)}, bf16[512,2048]{1,0:T(8,128)(2,1)S(1)}) custom-call(bf16[448,2048]{1,0:T(8,128)(2,1)} %stream.1, f32[2,2048]{1,0:T(2,128)} %gain.1, bf16[2,2048,256]{2,1,0:T(8,128)(2,1)} %wv.1, bf16[2,2048,256]{2,1,0:T(8,128)(2,1)} %wg.1, bf16[2,512,256]{2,1,0:T(8,128)(2,1)} %taps.1, ...), custom_call_target="tpu_custom_call" | custom-call | tf_op jit(solution)/shard_map/pallas_call | solution.py:425
  20.0 1.2 %shard_map.101 = bf16[448,2048]{1,0:T(8,128)(2,1)} custom-call(bf16[448,2048]{1,0:T(8,128)(2,1)S(1)} %get-tuple-element.8.x_v, bf16[128,512]{1,0:T(8,128)(2,1)S(1)} %get-tuple-element.9.mixed, bf16[512,2048]{1,0:T(8,128)(2,1)S(1)} %get-tuple-element.10.wo), custom_call_target="tpu_custom_call" | custom-call | tf_op jit(solution)/shard_map/pallas_call | solution.py:464

commit v3 on v2

--- a/solution.py
+++ b/solution.py
@@ -80,10 +80,11 @@
     other = pl.ds(pl.multiple_of((1 - tp) * half, half), half)
     first, second = pl.ds(0, half), pl.ds(half, half)
     loads = {}
+    free = list(range(load_sem.shape[0]))
     waited = set()
 
     def load(key, whole, *parts):
-        sem = load_sem.at[len(loads)]
+        sem = load_sem.at[free.pop(0)]
         loads[key] = pltpu.make_async_copy(whole, whole, sem)
         for source, target in parts:
             pltpu.make_async_copy(source, target, sem).start()
@@ -116,15 +117,18 @@
     load_rows("x0", head, x_v.shape[0])
     load_gate(0, STEPS)
     load_rows("x", 0, head)
-    load("taps", taps_v, (taps, taps_v))
-    load("mats", mats_v, (mats, mats_v))
-    load("bias", bias_v, (bias, bias_v))
-    load("cgain", cgain_v, (cgain.at[:, mine], cgain_v.at[:, first]), (cgain.at[:, other], cgain_v.at[:, second]))
-    load("cshift", cshift_v, (cshift.at[:, mine], cshift_v.at[:, first]), (cshift.at[:, other], cshift_v.at[:, second]))
-    for l in range(layers):
-        if l:
-            load_gate(l)
-        load_halves(("out", l), lambda channels: wo.at[l, channels], wo_last if l == layers - 1 else wo_v.at[l])
+    def load_rest():
+        free[:0] = range(2 + STEPS)
+        load("taps", taps_v, (taps, taps_v))
+        load("mats", mats_v, (mats, mats_v))
+        load("bias", bias_v, (bias, bias_v))
+        load("cgain", cgain_v, (cgain.at[:, mine], cgain_v.at[:, first]), (cgain.at[:, other], cgain_v.at[:, second]))
+        load("cshift", cshift_v, (cshift.at[:, mine], cshift_v.at[:, first]), (cshift.at[:, other], cshift_v.at[:, second]))
+        for l in range(layers):
+            if l:
+                load_gate(l)
+            load_halves(("out", l), lambda channels: wo.at[l, channels], wo_last if l == layers - 1 else wo_v.at[l])
+
     fwd_v, inv_v = mats_v.at[: 2 * BLOCK], mats_v.at[2 * BLOCK : 3 * BLOCK]
     oft_v = mats_v.at[3 * BLOCK :, :BLOCK]
 
@@ -228,7 +232,10 @@
     @scoped
     def spectrum(l, w):
         first, last = w * BLOCK, (w + 2) * BLOCK
-        spectra[l, w] = jnp.dot(fwd_v[...], gated[l, first:last, :], preferred_element_type=jnp.float32)
+        for half_bins in (slice(0, BLOCK), slice(BLOCK, 2 * BLOCK)):
+            spectra[l, w, half_bins, :] = jnp.dot(
+                fwd_v[half_bins, :], gated[l, first:last, :], preferred_element_type=jnp.float32
+            )
 
     summed = {}
 
@@ -358,6 +365,7 @@
     for c in range(plan.outs):
         gate(0, [c])
         if c == 0:
+            load_rest()
             with jax.named_scope("barrier"):
                 pl.semaphore_wait(barrier, 1 + jnp.minimum(plan.n_sp - 1 - sp, len(hops)))
         send(0, c)
@@ -449,7 +457,7 @@
             pltpu.VMEM((layers, tokens, half), bf16),
             pltpu.VMEM((layers, tokens, half), bf16),
             pltpu.VMEM((layers, tokens, LANES), f32),
-            dma((7 + STEPS + 2 * layers,)),
+            dma((max(3 + STEPS, 5 + 2 * layers),)),
             dma((n_hops,)),
             dma((layers, len(plan.slots))),
             dma((1,)),

time: 21.5 us -> 21.4 us (level)
  no operation moved by 1% of the time
where the time goes in v3:
time: 21.4 us; the launch traced here: 21.2 us
  Pallas kernels  21.2 us (99%)
    pallas_call x1, Pallas kernels, per_device(): pl.pallas_call(functools.partial(kernel, plan, layers), out_shape=[pltpu....  19.9 us
    pallas_call x1, Pallas kernels, per_device(): pl.pallas_call(functools.partial(last_out, done), out_shape=jax.ShapeDtyp...  1.22 us

profile of v3, /device:TPU:25, one launch (start us, length us, event | category | flops | bytes accessed | tf_op | source)
XLA Modules:
  0.0 21.2 jit_solution(3654218818374984858)
XLA Ops:
  0.0 19.9 %shard_map.100 = (bf16[448,2048]{1,0:T(8,128)(2,1)S(1)}, bf16[128,512]{1,0:T(8,128)(2,1)S(1)}, bf16[512,2048]{1,0:T(8,128)(2,1)S(1)}) custom-call(bf16[448,2048]{1,0:T(8,128)(2,1)} %stream.1, f32[2,2048]{1,0:T(2,128)} %gain.1, bf16[2,2048,256]{2,1,0:T(8,128)(2,1)} %wv.1, bf16[2,2048,256]{2,1,0:T(8,128)(2,1)} %wg.1, bf16[2,512,256]{2,1,0:T(8,128)(2,1)} %taps.1, ...), custom_call_target="tpu_custom_call" | custom-call | tf_op jit(solution)/shard_map/pallas_call | solution.py:433
  20.0 1.2 %shard_map.101 = bf16[448,2048]{1,0:T(8,128)(2,1)} custom-call(bf16[448,2048]{1,0:T(8,128)(2,1)S(1)} %get-tuple-element.8.x_v, bf16[128,512]{1,0:T(8,128)(2,1)S(1)} %get-tuple-element.9.mixed, bf16[512,2048]{1,0:T(8,128)(2,1)S(1)} %get-tuple-element.10.wo), custom_call_target="tpu_custom_call" | custom-call | tf_op jit(solution)/shard_map/pallas_call | solution.py:472

commit v4 on v3

--- a/solution.py
+++ b/solution.py
@@ -71,7 +71,7 @@
 def kernel(
     plan, layers, stream, gain, wv, wg, taps, bias, cgain, cshift, wo, mats, x_v, mixed_v, wo_last,
     gain_v, w_v, taps_v, bias_v, cgain_v, cshift_v, wo_v, mats_v,
-    gated, gained, spectra, kernels, sums, freq, conv, peer, shift, load_sem, send_sem, recv_sem, swap_send, swap_recv, fence_sem,
+    gated, gained, spectra, kernels, sums, freq, conv, peer, shift, load_sem, send_sem, recv_sem, swap_send, swap_recv,
 ):
     sp, tp = lax.axis_index("sp"), lax.axis_index("tp")
     half = wv.shape[2]
@@ -272,10 +272,6 @@
         for group in groups:
             for c in group:
                 add_ready(l, c)
-
-    def fence():
-        pl.semaphore_signal(fence_sem, 1)
-        pl.semaphore_wait(fence_sem, 1)
 
     def invert(l, c):
         a, b = plan.chunks[c]
@@ -349,10 +345,9 @@
         squares = 0.0
         for n in range(0, width, step):
             update = jnp.dot(mixed, out[:, n : n + step], preferred_element_type=jnp.float32)
-            new = (x_v[rows, n : n + step].astype(jnp.float32) + update).astype(jnp.bfloat16)
-            x_v[rows, n : n + step] = new
+            x = x_v[rows, n : n + step].astype(jnp.float32) + update
+            x_v[rows, n : n + step] = x.astype(jnp.bfloat16)
             if not last:
-                x = new.astype(jnp.float32)
                 squares = squares + jnp.sum(x * x, axis=-1, keepdims=True)
                 gained[rows, n : n + step] = (x * gain_v[l + 1 : l + 2, n : n + step]).astype(jnp.bfloat16)
         if not last:
@@ -385,7 +380,6 @@
                 convolve(l, group)
                 unmeaned = [group]
                 if which == [0]:
-                    fence()
                     add_later(l, plan.groups[1:])
             else:
                 finish(l, which, unmeaned)
@@ -462,7 +456,6 @@
             dma((layers, len(plan.slots))),
             dma((1,)),
             dma((layers, len(plan.groups))),
-            pltpu.SemaphoreType.REGULAR,
         ],
         compiler_params=pltpu.CompilerParams(
             collective_id=0, has_side_effects=True, vmem_limit_bytes=61300 * 1024

time: 21.4 us -> 21.4 us (level)
  no operation moved by 1% of the time
where the time goes in v4:
time: 21.4 us; the launch traced here: 21.2 us
  Pallas kernels  21.2 us (99%)
    pallas_call x1, Pallas kernels, per_device(): pl.pallas_call(functools.partial(kernel, plan, layers), out_shape=[pltpu....  19.9 us
    pallas_call x1, Pallas kernels, per_device(): pl.pallas_call(functools.partial(last_out, done), out_shape=jax.ShapeDtyp...  1.22 us

profile of v4, /device:TPU:25, one launch (start us, length us, event | category | flops | bytes accessed | tf_op | source)
XLA Modules:
  0.0 21.2 jit_solution(15443452582770591841)
XLA Ops:
  0.0 19.9 %shard_map.100 = (bf16[448,2048]{1,0:T(8,128)(2,1)S(1)}, bf16[128,512]{1,0:T(8,128)(2,1)S(1)}, bf16[512,2048]{1,0:T(8,128)(2,1)S(1)}) custom-call(bf16[448,2048]{1,0:T(8,128)(2,1)} %stream.1, f32[2,2048]{1,0:T(2,128)} %gain.1, bf16[2,2048,256]{2,1,0:T(8,128)(2,1)} %wv.1, bf16[2,2048,256]{2,1,0:T(8,128)(2,1)} %wg.1, bf16[2,512,256]{2,1,0:T(8,128)(2,1)} %taps.1, ...), custom_call_target="tpu_custom_call" | custom-call | tf_op jit(solution)/shard_map/pallas_call | solution.py:427
  20.0 1.2 %shard_map.101 = bf16[448,2048]{1,0:T(8,128)(2,1)} custom-call(bf16[448,2048]{1,0:T(8,128)(2,1)S(1)} %get-tuple-element.8.x_v, bf16[128,512]{1,0:T(8,128)(2,1)S(1)} %get-tuple-element.9.mixed, bf16[512,2048]{1,0:T(8,128)(2,1)S(1)} %get-tuple-element.10.wo), custom_call_target="tpu_custom_call" | custom-call | tf_op jit(solution)/shard_map/pallas_call | solution.py:465
